TPU v7x, 32 devices: a whole 2x2x4 slice. The times are simulated.
32 devices in a mesh: sp: 8 (over z, x), tp: 4 (over y, core).
Axes of the slice: x: 2, y: 2, z: 4, core: 2. Of those that a mesh axis runs over, the one named last changes fastest.
Arguments:
- queries: bfloat16 [4096, 1024], P('sp', 'tp'), may hold values from -5.5 to 5.5
- key_vectors: bfloat16 [4096, 1024], P('sp', 'tp'), may hold values from -5.5 to 5.5
- latents: bfloat16 [4096, 2048], P('sp', 'tp'), may hold values from -6 to 6
- w_value: bfloat16 [2048, 1024], P(None, 'tp'), may hold values from -0.125 to 0.125
- log_sums: float32 [4096, 16], P('sp', 'tp'), as said below
- out_pair: bfloat16 [4096, 2048], P('sp', 'tp'), may hold values from -6 to 6
- cotangent: bfloat16 [4096, 1024], P('sp', 'tp'), may hold values from -6 to 6
- lambdas: float32 [8], P('tp'), may hold values from 0.3 to 0.8
- out_gain: float32 [128], replicated, may hold values from 0.1 to 1.9
Outputs:
- query_grad: float32 [4096, 1024], P('sp', 'tp')
- key_grad: float32 [4096, 1024], P('sp', 'tp')
- value_grad: float32 [4096, 1024], P('sp', 'tp')
- weight_grad: float32 [2048, 1024], P('sp', 'tp')
Inputs may be any that keep to these rules, and one draw needn't show every extreme that they name: `log_sums`: each entry is the logarithm of the sum of exp(scores_c[t, s]) over s <= t for its row t, head h and map c.
All inputs are finite; a program needn't handle non-finite values.
Results may differ from a plain program's by a relative error of at most 0.008.
Values may be sent and summed in bfloat16 or wider, within the bound.
A program may use at most 64 MiB of HBM per device.

v0:
```python
import jax
import jax.numpy as jnp
from jax import lax
from jax.sharding import PartitionSpec as P

norm_floor = 0.25
block_rows = 512


def head_cotangent(out_pair, cotangent, lambdas, out_gain):
    tok_rows = out_pair.shape[0]
    head_count = lambdas.shape[0]
    out_maps = out_pair.astype(jnp.float32).reshape(tok_rows, head_count, 2, -1)
    lam_cols = lambdas[None, :, None]
    merged = out_maps[:, :, 0] - lam_cols * out_maps[:, :, 1]
    inv_norm = lax.rsqrt(jnp.mean(merged * merged, axis=-1, keepdims=True) + norm_floor)
    scaled = cotangent.astype(jnp.float32).reshape(merged.shape) * out_gain
    inner_dot = jnp.mean(scaled * merged, axis=-1, keepdims=True)
    out_grad = (inv_norm * scaled - merged * (inv_norm * inv_norm * inv_norm) * inner_dot).astype(
        jnp.bfloat16
    )
    grad_wide = out_grad.astype(jnp.float32)
    first_map = jnp.sum(grad_wide * out_maps[:, :, 0], axis=-1)
    second_map = -lambdas[None, :] * jnp.sum(grad_wide * out_maps[:, :, 1], axis=-1)
    return (out_grad, jnp.stack([first_map, second_map], axis=-1))


def block_terms(
    query_block,
    key_block,
    value_block,
    grad_block,
    log_block,
    term_block,
    lambdas,
    query_pos,
    key_pos,
):
    factor = query_block.shape[-1] ** (-0.5)
    scores = (
        jnp.einsum("qhcd,khcd->hcqk", query_block, key_block, preferred_element_type=jnp.float32)
        * factor
    )
    visible = key_pos[None, :] <= query_pos[:, None]
    shifted = scores - jnp.transpose(log_block, (1, 2, 0))[..., None]
    softmax_maps = jnp.where(visible, jnp.exp(shifted), 0.0)
    value_dot = jnp.einsum(
        "qhe,khe->hqk", grad_block, value_block, preferred_element_type=jnp.float32
    )
    lam_cols = lambdas[:, None, None]
    weights = (softmax_maps[:, 0] - lam_cols * softmax_maps[:, 1]).astype(jnp.bfloat16)
    term_cols = jnp.transpose(term_block, (1, 2, 0))
    first_map = softmax_maps[:, 0] * (value_dot - term_cols[:, 0, :, None])
    second_map = softmax_maps[:, 1] * (-lam_cols * value_dot - term_cols[:, 1, :, None])
    dscore = (jnp.stack([first_map, second_map], axis=1) * factor).astype(jnp.bfloat16)
    return (weights, dscore)


def block_span():
    return block_rows


def per_device(
    queries, key_vectors, latents, w_value, log_sums, out_pair, cotangent, lambdas, out_gain
):
    tok_rows = queries.shape[0]
    head_count = lambdas.shape[0]
    offset = lax.axis_index("sp") * tok_rows
    own_pos = offset + jnp.arange(tok_rows, dtype=jnp.int32)
    last_pos = offset + tok_rows - 1
    gathered = lax.all_gather(latents, "tp", axis=1, tiled=True)
    values = jnp.dot(gathered, w_value, preferred_element_type=jnp.float32).astype(jnp.bfloat16)
    out_grad, row_terms = head_cotangent(out_pair, cotangent, lambdas, out_gain)
    query_heads = queries.reshape(tok_rows, head_count, 2, -1)
    key_heads = key_vectors.reshape(tok_rows, head_count, 2, -1)
    value_heads = values.reshape(tok_rows, head_count, -1)
    log_heads = log_sums.reshape(tok_rows, head_count, 2)
    grad_flat = out_grad.reshape(tok_rows, -1)
    term_flat = row_terms.reshape(tok_rows, -1)
    zero_keys = jnp.zeros(key_heads.shape, jnp.float32)
    zero_values = jnp.zeros(value_heads.shape, jnp.float32)
    shards = (
        lax.all_gather(key_vectors, "sp", axis=0, tiled=True),
        lax.all_gather(values, "sp", axis=0, tiled=True),
    )
    key_piece = shards[0]
    value_piece = shards[1]
    piece_rows = key_piece.shape[0]
    block_len = block_span()

    def query_add_block(block_idx, partial_value):
        begin_row = block_idx * block_len
        key_block = lax.dynamic_slice_in_dim(key_piece, begin_row, block_len, 0).reshape(
            block_len, head_count, 2, -1
        )
        value_block = lax.dynamic_slice_in_dim(value_piece, begin_row, block_len, 0).reshape(
            block_len, head_count, -1
        )
        key_pos = begin_row + jnp.arange(block_len, dtype=jnp.int32)

        def query_compute(sums):
            weights, dscore = block_terms(
                query_heads,
                key_block,
                value_block,
                out_grad,
                log_heads,
                row_terms,
                lambdas,
                own_pos,
                key_pos,
            )
            return sums + jnp.einsum(
                "hcqk,khcd->qhcd", dscore, key_block, preferred_element_type=jnp.float32
            )

        return lax.cond(begin_row <= last_pos, query_compute, lambda sums: sums, partial_value)

    query_grad = lax.fori_loop(0, piece_rows // block_len, query_add_block, zero_keys)
    shards = (
        lax.all_gather(queries.astype(jnp.float32), "sp", axis=0, tiled=True).astype(jnp.bfloat16),
        lax.all_gather(grad_flat.astype(jnp.float32), "sp", axis=0, tiled=True).astype(
            jnp.bfloat16
        ),
        lax.all_gather(log_sums, "sp", axis=0, tiled=True),
        lax.all_gather(term_flat, "sp", axis=0, tiled=True),
    )
    query_piece = shards[0]
    grad_piece = shards[1]
    log_piece = shards[2]
    term_piece = shards[3]
    piece_rows = query_piece.shape[0]
    key_block_len = block_span()

    def key_add_block(block_idx, partial_value):
        begin_row = block_idx * key_block_len
        query_block = lax.dynamic_slice_in_dim(query_piece, begin_row, key_block_len, 0).reshape(
            key_block_len, head_count, 2, -1
        )
        grad_block = lax.dynamic_slice_in_dim(grad_piece, begin_row, key_block_len, 0).reshape(
            key_block_len, head_count, -1
        )
        log_block = lax.dynamic_slice_in_dim(log_piece, begin_row, key_block_len, 0).reshape(
            key_block_len, head_count, 2
        )
        term_block = lax.dynamic_slice_in_dim(term_piece, begin_row, key_block_len, 0).reshape(
            key_block_len, head_count, 2
        )
        query_pos = begin_row + jnp.arange(key_block_len, dtype=jnp.int32)

        def key_compute(sums):
            weights, dscore = block_terms(
                query_block,
                key_heads,
                value_heads,
                grad_block,
                log_block,
                term_block,
                lambdas,
                query_pos,
                own_pos,
            )
            key_sum = sums[0] + jnp.einsum(
                "hcqk,qhcd->khcd", dscore, query_block, preferred_element_type=jnp.float32
            )
            value_sum = sums[1] + jnp.einsum(
                "hqk,qhe->khe", weights, grad_block, preferred_element_type=jnp.float32
            )
            return (key_sum, value_sum)

        return lax.cond(
            begin_row + key_block_len - 1 >= offset, key_compute, lambda sums: sums, partial_value
        )

    key_grad, value_grad = lax.fori_loop(
        0, piece_rows // key_block_len, key_add_block, (zero_keys, zero_values)
    )
    value_flat = value_grad.reshape(tok_rows, -1)
    value_narrow = value_flat.astype(jnp.bfloat16)
    weight_grad = lax.psum_scatter(
        lax.dot_general(
            gathered, value_narrow, (((0,), (0,)), ((), ())), preferred_element_type=jnp.float32
        ),
        "sp",
        scatter_dimension=0,
        tiled=True,
    )
    return (
        query_grad.reshape(tok_rows, -1),
        key_grad.reshape(tok_rows, -1),
        value_flat,
        weight_grad,
    )


def solution(mesh):
    return jax.shard_map(
        per_device,
        mesh=mesh,
        in_specs=(
            P("sp", "tp"),
            P("sp", "tp"),
            P("sp", "tp"),
            P(None, "tp"),
            P("sp", "tp"),
            P("sp", "tp"),
            P("sp", "tp"),
            P("tp"),
            P(),
        ),
        out_specs=(P("sp", "tp"), P("sp", "tp"), P("sp", "tp"), P("sp", "tp")),
        check_vma=False,
    )
```

profile of v0, /device:TPU:0, one launch (start us, length us, event | category | flops | bytes accessed | tf_op | source)
XLA Modules:
  0.0 320.5 jit_solution(6820730226512585887)
XLA Ops:
  14.8 20.2 %all-gather.8.cloned.1.call-done = bf16[512,2048]{1,0:T(8,128)(2,1)} async-done(((bf16[512,512]{1,0:T(8,128)(2,1)}), bf16[512,2048]{1,0:T(8,128)(2,1)}) %all-gather.8.cloned.1.call-update) | async-done | bytes 2097168 | tf_op jit(solution)/shard_map/all_gather | solution.py:71
  34.9 3.1 convolution_convert_fusion
  38.7 31.0 %all_gather.25 = f32[4096,4]{0,1:T(4,128)S(1)} all-gather(f32[512,4]{0,1:T(4,128)S(1)} %copy-done.6), channel_id=1, replica_groups=mesh['sp'=8,'tp'=4] {'sp'}, dimensions={0}, use_global_device_ids=true | all-gather | bytes 73728 | tf_op jit(solution)/shard_map/all_gather | solution.py:125
  69.7 31.9 %all_gather.27 = f32[4096,4]{0,1:T(4,128)} all-gather(f32[512,4]{0,1:T(4,128)S(1)} %reshape.188), channel_id=1, replica_groups=mesh['sp'=8,'tp'=4] {'sp'}, dimensions={0}, use_global_device_ids=true | all-gather | bytes 73728 | tf_op jit(solution)/shard_map/all_gather | solution.py:126
  102.8 37.0 %all-gather.14.cloned.1.call-done = bf16[4096,256]{0,1:T(8,128)(2,1)} async-done(((bf16[512,256]{0,1:T(8,128)(2,1)}), bf16[4096,256]{0,1:T(8,128)(2,1)}) %all-gather.14.cloned.1.call-update) | async-done | bytes 2097168 | tf_op jit(solution)/shard_map/all_gather | solution.py:122
  139.9 90.7 %while.39 = (s32[]{:T(128)}, f32[512,2,2,64]{0,3,2,1:T(8,128)S(1)}, f32[512,2,128]{2,0,1:T(8,128)S(1)}, s32[]{:T(128)}, bf16[4096,256]{0,1:T(8,128)(2,1)}, /*ind...) while((s32[]{:T(128)}, f32[512,2,2,64]{0,3,2,1:T(8,128)S(1)}, ...), condition=%wide.region_11.12_spmd.clone.clone, body=%wide.region_8.11_spmd.clone.clone.sunk | while | flops 547881984 | bytes 43121072 | solution.py:175
  140.0 11.3 %conditional.8 = ((f32[512,2,2,64]{0,3,2,1:T(8,128)S(1)}, f32[512,2,128]{2,0,1:T(8,128)S(1)})) conditional(s32[]{:T(128)} %convert_element_type.110, (f32[512,2,2,64]{0,3,2,1:T(8,128)S(1)}, f32[512,2,128]{2,0,1:T(8,128)S(1)}) %tuple.152, (s32[]{:T(128)}, s32[]{:T(128)}, s32[512]{0:T(512)S(1)}, bf16[4096,256]{0,1:T(8,128)(2,1)}, ...), branch_computations={%region_9.9_spmd, %region_10.10_spmd} | conditional | flops 547881984 | bytes 43118728 | solution.py:171
  142.0 3.2 exponential_select_fusion
  145.2 2.9 multiply_bitcast_fusion.1
  151.3 11.3 %conditional.8 = ((f32[512,2,2,64]{0,3,2,1:T(8,128)S(1)}, f32[512,2,128]{2,0,1:T(8,128)S(1)})) conditional(s32[]{:T(128)} %convert_element_type.110, (f32[512,2,2,64]{0,3,2,1:T(8,128)S(1)}, f32[512,2,128]{2,0,1:T(8,128)S(1)}) %tuple.152, (s32[]{:T(128)}, s32[]{:T(128)}, s32[512]{0:T(512)S(1)}, bf16[4096,256]{0,1:T(8,128)(2,1)}, ...), branch_computations={%region_9.9_spmd, %region_10.10_spmd} | conditional | flops 547881984 | bytes 43118728 | solution.py:171
  153.4 3.2 exponential_select_fusion
  162.6 11.4 %conditional.8 = ((f32[512,2,2,64]{0,3,2,1:T(8,128)S(1)}, f32[512,2,128]{2,0,1:T(8,128)S(1)})) conditional(s32[]{:T(128)} %convert_element_type.110, (f32[512,2,2,64]{0,3,2,1:T(8,128)S(1)}, f32[512,2,128]{2,0,1:T(8,128)S(1)}) %tuple.152, (s32[]{:T(128)}, s32[]{:T(128)}, s32[512]{0:T(512)S(1)}, bf16[4096,256]{0,1:T(8,128)(2,1)}, ...), branch_computations={%region_9.9_spmd, %region_10.10_spmd} | conditional | flops 547881984 | bytes 43118728 | solution.py:171
  164.7 3.2 exponential_select_fusion
  167.9 3.1 multiply_bitcast_fusion.1
  174.1 11.3 %conditional.8 = ((f32[512,2,2,64]{0,3,2,1:T(8,128)S(1)}, f32[512,2,128]{2,0,1:T(8,128)S(1)})) conditional(s32[]{:T(128)} %convert_element_type.110, (f32[512,2,2,64]{0,3,2,1:T(8,128)S(1)}, f32[512,2,128]{2,0,1:T(8,128)S(1)}) %tuple.152, (s32[]{:T(128)}, s32[]{:T(128)}, s32[512]{0:T(512)S(1)}, bf16[4096,256]{0,1:T(8,128)(2,1)}, ...), branch_computations={%region_9.9_spmd, %region_10.10_spmd} | conditional | flops 547881984 | bytes 43118728 | solution.py:171
  176.1 3.2 exponential_select_fusion
  185.4 11.2 %conditional.8 = ((f32[512,2,2,64]{0,3,2,1:T(8,128)S(1)}, f32[512,2,128]{2,0,1:T(8,128)S(1)})) conditional(s32[]{:T(128)} %convert_element_type.110, (f32[512,2,2,64]{0,3,2,1:T(8,128)S(1)}, f32[512,2,128]{2,0,1:T(8,128)S(1)}) %tuple.152, (s32[]{:T(128)}, s32[]{:T(128)}, s32[512]{0:T(512)S(1)}, bf16[4096,256]{0,1:T(8,128)(2,1)}, ...), branch_computations={%region_9.9_spmd, %region_10.10_spmd} | conditional | flops 547881984 | bytes 43118728 | solution.py:171
  187.4 3.2 exponential_select_fusion
  196.7 11.3 %conditional.8 = ((f32[512,2,2,64]{0,3,2,1:T(8,128)S(1)}, f32[512,2,128]{2,0,1:T(8,128)S(1)})) conditional(s32[]{:T(128)} %convert_element_type.110, (f32[512,2,2,64]{0,3,2,1:T(8,128)S(1)}, f32[512,2,128]{2,0,1:T(8,128)S(1)}) %tuple.152, (s32[]{:T(128)}, s32[]{:T(128)}, s32[512]{0:T(512)S(1)}, bf16[4096,256]{0,1:T(8,128)(2,1)}, ...), branch_computations={%region_9.9_spmd, %region_10.10_spmd} | conditional | flops 547881984 | bytes 43118728 | solution.py:171
  198.7 3.2 exponential_select_fusion
  202.0 2.9 multiply_bitcast_fusion.1
  208.0 11.2 %conditional.8 = ((f32[512,2,2,64]{0,3,2,1:T(8,128)S(1)}, f32[512,2,128]{2,0,1:T(8,128)S(1)})) conditional(s32[]{:T(128)} %convert_element_type.110, (f32[512,2,2,64]{0,3,2,1:T(8,128)S(1)}, f32[512,2,128]{2,0,1:T(8,128)S(1)}) %tuple.152, (s32[]{:T(128)}, s32[]{:T(128)}, s32[512]{0:T(512)S(1)}, bf16[4096,256]{0,1:T(8,128)(2,1)}, ...), branch_computations={%region_9.9_spmd, %region_10.10_spmd} | conditional | flops 547881984 | bytes 43118728 | solution.py:171
  210.1 3.2 exponential_select_fusion
  213.3 2.9 multiply_bitcast_fusion.1
  219.3 11.3 %conditional.8 = ((f32[512,2,2,64]{0,3,2,1:T(8,128)S(1)}, f32[512,2,128]{2,0,1:T(8,128)S(1)})) conditional(s32[]{:T(128)} %convert_element_type.110, (f32[512,2,2,64]{0,3,2,1:T(8,128)S(1)}, f32[512,2,128]{2,0,1:T(8,128)S(1)}) %tuple.152, (s32[]{:T(128)}, s32[]{:T(128)}, s32[512]{0:T(512)S(1)}, bf16[4096,256]{0,1:T(8,128)(2,1)}, ...), branch_computations={%region_9.9_spmd, %region_10.10_spmd} | conditional | flops 547881984 | bytes 43118728 | solution.py:171
  221.4 3.2 exponential_select_fusion
  224.6 3.0 multiply_bitcast_fusion.1
  230.7 3.9 %convolution_bitcast_fusion.1 = f32[2048,256]{0,1:T(8,128)} fusion(bf16[512,2048]{1,0:T(8,128)(2,1)} %all-gather.8.cloned.1.call-done, f32[512,256]{1,0:T(8,128)S(1)} %copy_bitcast_fusion.2), kind=kOutput, calls=%fused_computation.46 | convolution fusion | flops 537001984 | bytes 4718592 | tf_op jit(solution)/shard_map/dot_general | solution.py:181
  235.8 5.5 %all-gather.10.cloned.1.call-done = bf16[4096,256]{0,1:T(8,128)(2,1)} async-done(((bf16[512,256]{0,1:T(8,128)(2,1)}), bf16[4096,256]{0,1:T(8,128)(2,1)}) %all-gather.10.cloned.1.call-update) | async-done | bytes 2097168 | tf_op jit(solution)/shard_map/all_gather | solution.py:84
  241.4 4.3 %while.38 = (s32[]{:T(128)}, f32[512,2,2,64]{0,3,2,1:T(8,128)S(1)}, s32[]{:T(128)}, bf16[4096,256]{0,1:T(8,128)(2,1)}, bf16[512,2,2,64]{0,3,2,1:T(8,128)(2,1)S(1...) while((s32[]{:T(128)}, f32[512,2,2,64]{0,3,2,1:T(8,128)S(1)}, ...), condition=%wide.region_7.8_spmd.clone, body=%wide.region_4.7_spmd.clone.sunk | while | flops 411960320 | bytes 20756812 | solution.py:119
  241.4 3.9 %conditional.7 = (f32[512,2,2,64]{0,3,2,1:T(8,128)S(1)}) conditional(s32[]{:T(128)} %convert_element_type.109, f32[512,2,2,64]{0,3,2,1:T(8,128)S(1)} %get-tuple-element.1245, (s32[]{:T(128)}, s32[512]{0:T(512)S(1)}, s32[]{:T(128)}, bf16[4096,256]{0,1:T(8,128)(2,1)}, bf16[512,2,2,64]{0,3,2,1:T(8,128)(2,1)S(1)}, /*index=5*/f32[512,2,2]{0,2,1:T(2,128)S(1)}, ...), branch_computations={%region_5.0_spmd, %region_6.6_spmd} | conditional | flops 411960320 | bytes 20754510 | solution.py:117
  246.7 65.2 %reduce-scatter.2.cloned.1.call-done = f32[256,256]{0,1:T(8,128)} async-done(((f32[2048,256]{0,1:T(8,128)}), f32[256,256]{0,1:T(8,128)}) %reduce-scatter.2.cloned.1.call-update) | async-done | bytes 262160 | tf_op jit(solution)/shard_map/reduce_scatter | solution.py:180
  (202 shorter events, 66.7 us)
Async XLA Ops:
  7.2 27.7 %copy-start = (bf16[2048,256]{1,0:T(8,128)(2,1)S(1)}, bf16[2048,256]{1,0:T(8,128)(2,1)}, u32[]{:S(2)}) copy-start(bf16[2048,256]{1,0:T(8,128)(2,1)} %param.20) | copy-start | bytes 3145732
  7.2 3.9 %copy-start.5 = (bf16[512,256]{1,0:T(8,128)(2,1)S(1)}, bf16[512,256]{1,0:T(8,128)(2,1)}, u32[]{:S(2)}) copy-start(bf16[512,256]{1,0:T(8,128)(2,1)} %param.23) | copy-start | bytes 786436
  7.2 4.1 %copy-start.8 = (f32[128]{0:T(128)S(1)}, f32[128]{0:T(128)}, u32[]{:S(2)}) copy-start(f32[128]{0:T(128)} %param.25) | copy-start | bytes 1540
  7.2 4.1 %copy-start.7 = (f32[2]{0:T(128)S(1)}, f32[2]{0:T(128)}, u32[]{:S(2)}) copy-start(f32[2]{0:T(128)} %param.24) | copy-start | bytes 28
  7.2 27.7 %all-gather.8.cloned.1.call-start = ((), (), s32[]{:S(2)}) async-start(), calls=%async_computation.2 | async-start | bytes 2621440 | tf_op jit(solution)/shard_map/all_gather | solution.py:71
  7.9 94.8 %all-gather.12.cloned.1.call-start = ((), (), s32[]{:S(2)}) async-start(), calls=%async_computation.4 | async-start | bytes 2359296 | tf_op jit(solution)/shard_map/all_gather | solution.py:121
  9.8 130.0 %all-gather.14.cloned.1.call-start = ((), (), s32[]{:S(2)}) async-start(), calls=%async_computation.5 | async-start | bytes 2359296 | tf_op jit(solution)/shard_map/all_gather | solution.py:122
  12.8 222.9 %all-gather.6.cloned.1.call-start = ((), (), s32[]{:S(2)}) async-start(), calls=%async_computation.1 | async-start | bytes 2359296 | tf_op jit(solution)/shard_map/all_gather | solution.py:83
  14.7 226.6 %all-gather.10.cloned.1.call-start = ((), (), s32[]{:S(2)}) async-start(), calls=%async_computation.3 | async-start | bytes 2359296 | tf_op jit(solution)/shard_map/all_gather | solution.py:84
  38.0 0.7 copy-start.6
  38.0 101.9 %copy-start.4 = (bf16[512,256]{0,1:T(8,128)(2,1)S(1)}, bf16[512,256]{0,1:T(8,128)(2,1)}, u32[]{:S(2)}) copy-start(bf16[512,256]{0,1:T(8,128)(2,1)} %copy.47) | copy-start | bytes 786436
  38.0 273.8 %reduce-scatter.2.cloned.1.call-start = ((), (), s32[]{:S(2)}) async-start(), calls=%async_computation.6 | async-start | bytes 2359296 | tf_op jit(solution)/shard_map/reduce_scatter | solution.py:180
  148.2 2.3 copy-start.1
  159.6 2.2 copy-start.1
  171.0 2.2 copy-start.1
  182.3 2.2 copy-start.1
  193.6 2.2 copy-start.1
  204.9 2.2 copy-start.1
  216.2 2.2 copy-start.1
  227.6 2.2 copy-start.1
  230.7 3.9 %copy-start.2 = (f32[512,256]{1,0:T(8,128)}, f32[512,256]{1,0:T(8,128)S(1)}, u32[]{:S(2)}) copy-start(f32[512,256]{1,0:T(8,128)S(1)} %copy_bitcast_fusion.2) | copy-start | bytes 1572868
  234.6 6.8 %copy-start.3 = (bf16[512,256]{0,1:T(8,128)(2,1)S(1)}, bf16[512,256]{0,1:T(8,128)(2,1)}, u32[]{:S(2)}) copy-start(bf16[512,256]{0,1:T(8,128)(2,1)} %copy.48) | copy-start | bytes 786436
Sparse Core Ops, SparseCore 0:
  9.6 25.2 all-gather.7
  37.5 50.9 all-gather.11
  91.1 48.6 all-gather.13
  142.3 48.5 all-gather.5
  192.7 48.5 all-gather.9
  244.7 67.0 reduce-scatter.1
where the time goes:
time: 322 us; the launch traced here: 320 us
  waiting for transfers between devices  129 us (40%)
  matrix products  69.3 us (22%)
  blocking collectives  62.9 us (20%)
  local copies, waits for them, and re-layouts  39.8 us (12%)
  between operations  14.3 us (4%)
  other arithmetic  3.63 us (1%)
    reduce_scatter x1, waiting for transfers between devices, per_device(): lax.psum_scatter(lax.dot_general(gathered, value_narrow, (((0,), (0,)), (...  65.2 us
    all_gather x1, waiting for transfers between devices, per_device(): lax.all_gather(grad_flat.astype(jnp.float32), 'sp', axis=0, tiled=True)  37 us
    all_gather x1, blocking collectives, per_device(): lax.all_gather(term_flat, 'sp', axis=0, tiled=True)  31.9 us
    all_gather x1, blocking collectives, per_device(): lax.all_gather(log_sums, 'sp', axis=0, tiled=True)  31 us
    dot_general x9, matrix products, block_terms(): jnp.einsum('qhcd,khcd->hcqk', query_block, key_block, preferred_element_t...  26.6 us
    dot_general x9, matrix products, block_terms(): jnp.einsum('qhe,khe->hqk', grad_block, value_block, preferred_element_typ...  24.4 us
    all_gather x1, waiting for transfers between devices, per_device(): gathered = lax.all_gather(latents, 'tp', axis=1, tiled=True)  20.2 us
    cond x32, local copies, waits for them, and re-layouts  13.3 us
  transfers between devices with their start and end apart: 6, of which 4 were waited for; matrix products, arithmetic and copies ran while one was open for 30% of the time, Pallas kernels for 0%

commit v1 on v0

--- a/solution.py
+++ b/solution.py
@@ -1,3 +1,4 @@
+import functools
 import jax
 import jax.numpy as jnp
 from jax import lax
@@ -5,6 +6,21 @@
 
 norm_floor = 0.25
 block_rows = 512
+
+
+def _solve_bands(inner_x, across, in_dim):
+    return jnp.concatenate(
+        lax.all_to_all(
+            jnp.stack([inner_x] * lax.axis_size(across), 0),
+            axis_name=across,
+            split_axis=0,
+            concat_axis=0,
+        ),
+        axis=in_dim,
+    )
+
+
+update_orders = functools.partial(_solve_bands, across="tp", in_dim=1)
 
 
 def head_cotangent(out_pair, cotangent, lambdas, out_gain):
@@ -68,7 +84,7 @@
     offset = lax.axis_index("sp") * tok_rows
     own_pos = offset + jnp.arange(tok_rows, dtype=jnp.int32)
     last_pos = offset + tok_rows - 1
-    gathered = lax.all_gather(latents, "tp", axis=1, tiled=True)
+    gathered = update_orders(latents)
     values = jnp.dot(gathered, w_value, preferred_element_type=jnp.float32).astype(jnp.bfloat16)
     out_grad, row_terms = head_cotangent(out_pair, cotangent, lambdas, out_gain)
     query_heads = queries.reshape(tok_rows, head_count, 2, -1)

time: 322 us -> 297 us (0.922)
  waiting for transfers between devices: 129 us -> 77.4 us
  blocking collectives: 62.9 us -> 91.8 us
    all_gather x1, waiting for transfers between devices: 37 us -> 2.82 us  [per_device(): lax.all_gather(grad_flat.astype(jnp.float32), 'sp', axis=0, tiled=True)]
    all_to_all x0 -> x1, blocking collectives: none -> 29.7 us  [_solve_bands(): lax.all_to_all(jnp.stack([inner_x] * lax.axis_size(across), 0), axis_name...]
    all_gather x1 -> x0, waiting for transfers between devices: 20.2 us -> none  [per_device(): gathered = lax.all_gather(latents, 'tp', axis=1, tiled=True)]
    dynamic_slice x8, local copies, waits for them, and re-layouts: 5.66 us -> 0.09 us  [key_add_block(): lax.dynamic_slice_in_dim(term_piece, begin_row, key_block_len, 0)]
    all_gather x1, waiting for transfers between devices: 5.54 us -> 9.21 us  [per_device(): lax.all_gather(values, 'sp', axis=0, tiled=True)]
    unnamed x25 -> x30, local copies, waits for them, and re-layouts: 10.3 us -> 13.7 us
    cond x32 -> x48, local copies, waits for them, and re-layouts: 13.3 us -> 13.4 us
  transfers between devices with their start and end apart: 6 -> 5, of which waited for: 4 -> 3; matrix products, arithmetic and copies ran while one was open for 30% -> 31% of each run, Pallas kernels for 0% -> 0%
where the time goes in v1:
time: 297 us; the launch traced here: 296 us
  blocking collectives  91.8 us (31%)
  waiting for transfers between devices  77.4 us (26%)
  matrix products  67.7 us (23%)
  local copies, waits for them, and re-layouts  38.7 us (13%)
  between operations  14 us (5%)
  other arithmetic  4.34 us (1%)
    reduce_scatter x1, waiting for transfers between devices, per_device(): lax.psum_scatter(lax.dot_general(gathered, value_narrow, (((0,), (0,)), (...  65.2 us
    all_gather x1, blocking collectives, per_device(): lax.all_gather(log_sums, 'sp', axis=0, tiled=True)  31.2 us
    all_gather x1, blocking collectives, per_device(): lax.all_gather(term_flat, 'sp', axis=0, tiled=True)  30.9 us
    all_to_all x1, blocking collectives, _solve_bands(): lax.all_to_all(jnp.stack([inner_x] * lax.axis_size(across), 0), axis_name...  29.7 us
    dot_general x9, matrix products, block_terms(): jnp.einsum('qhcd,khcd->hcqk', query_block, key_block, preferred_element_t...  26.7 us
    dot_general x9, matrix products, block_terms(): jnp.einsum('qhe,khe->hqk', grad_block, value_block, preferred_element_typ...  24.5 us
    unnamed x30, local copies, waits for them, and re-layouts  13.7 us
    cond x48, local copies, waits for them, and re-layouts  13.4 us
  transfers between devices with their start and end apart: 5, of which 3 were waited for; matrix products, arithmetic and copies ran while one was open for 31% of the time, Pallas kernels for 0%

profile of v1, /device:TPU:0, one launch (start us, length us, event | category | flops | bytes accessed | tf_op | source)
XLA Modules:
  0.0 296.0 jit_solution(5063968905553990007)
XLA Ops:
  16.5 29.7 %all_to_all.5 = bf16[4,512,512]{1,2,0:T(8,128)(2,1)S(1)} all-to-all(bf16[4,512,512]{1,2,0:T(8,128)(2,1)S(1)} %stack.50), channel_id=1, replica_groups=mesh['sp'=8,'tp'=4] {'tp'}, dimensions={0} | all-to-all | bytes 4194304 | tf_op jit(solution)/shard_map/all_to_all | solution.py:13
  50.2 31.2 %all_gather.21 = f32[4096,4]{0,1:T(4,128)S(1)} all-gather(f32[512,4]{0,1:T(4,128)S(1)} %copy-done.7), channel_id=1, replica_groups=mesh['sp'=8,'tp'=4] {'sp'}, dimensions={0}, use_global_device_ids=true | all-gather | bytes 73728 | tf_op jit(solution)/shard_map/all_gather | solution.py:141
  81.4 30.9 %all_gather.23 = f32[4096,4]{0,1:T(4,128)S(1)} all-gather(f32[512,4]{0,1:T(4,128)S(1)} %reshape.199), channel_id=1, replica_groups=mesh['sp'=8,'tp'=4] {'sp'}, dimensions={0}, use_global_device_ids=true | all-gather | bytes 73728 | tf_op jit(solution)/shard_map/all_gather | solution.py:142
  115.4 85.6 %while.39 = (s32[]{:T(128)}, f32[512,2,2,64]{0,3,2,1:T(8,128)S(1)}, f32[512,2,128]{2,0,1:T(8,128)S(1)}, s32[]{:T(128)}, bf16[4096,256]{0,1:T(8,128)(2,1)}, /*ind...) while((s32[]{:T(128)}, f32[512,2,2,64]{0,3,2,1:T(8,128)S(1)}, ...), condition=%wide.region_11.12_spmd.clone.clone, body=%wide.region_8.11_spmd.clone.clone.sunk | while | flops 547881984 | bytes 43121128 | solution.py:191
  115.5 10.7 %conditional.8 = ((f32[512,2,2,64]{0,3,2,1:T(8,128)S(1)}, f32[512,2,128]{2,0,1:T(8,128)S(1)})) conditional(s32[]{:T(128)} %convert_element_type.112, (f32[512,2,2,64]{0,3,2,1:T(8,128)S(1)}, f32[512,2,128]{2,0,1:T(8,128)S(1)}) %tuple.152, (s32[]{:T(128)}, s32[]{:T(128)}, s32[512]{0:T(512)S(1)}, bf16[4096,256]{0,1:T(8,128)(2,1)}, ...), branch_computations={%region_9.9_spmd, %region_10.10_spmd} | conditional | flops 547881984 | bytes 43118784 | solution.py:187
  116.9 3.2 %exponential_select_fusion = f32[2,2,512,512]{3,2,1,0:T(8,128)} fusion(bf16[512,2,2,64]{0,3,2,1:T(8,128)(2,1)S(1)} %bitcast.178, bf16[512,2,2,64]{0,3,2,1:T(8,128)(2,1)S(1)} %get-tuple-element.842, f32[2,2,512]{2,1,0:T(2,128)S(1)} %bitcast.192, pred[512,512]{1,0:T(8,128)(4,1)S(1)} %broadcast_compare_fusion.1), kind=kOutput, calls=%fused_computation.24 | convolution fusion | flops 137363456 | bytes 4988928 | tf_op jit(solution)/shard_map/while/body/eval_jaxpr/cond/branch_1_fun/qhcd,khcd->hcqk/dot_general | solution.py:57
  120.1 2.9 multiply_bitcast_fusion.1
  126.2 10.6 %conditional.8 = ((f32[512,2,2,64]{0,3,2,1:T(8,128)S(1)}, f32[512,2,128]{2,0,1:T(8,128)S(1)})) conditional(s32[]{:T(128)} %convert_element_type.112, (f32[512,2,2,64]{0,3,2,1:T(8,128)S(1)}, f32[512,2,128]{2,0,1:T(8,128)S(1)}) %tuple.152, (s32[]{:T(128)}, s32[]{:T(128)}, s32[512]{0:T(512)S(1)}, bf16[4096,256]{0,1:T(8,128)(2,1)}, ...), branch_computations={%region_9.9_spmd, %region_10.10_spmd} | conditional | flops 547881984 | bytes 43118784 | solution.py:187
  127.6 3.2 %exponential_select_fusion = f32[2,2,512,512]{3,2,1,0:T(8,128)} fusion(bf16[512,2,2,64]{0,3,2,1:T(8,128)(2,1)S(1)} %bitcast.178, bf16[512,2,2,64]{0,3,2,1:T(8,128)(2,1)S(1)} %get-tuple-element.842, f32[2,2,512]{2,1,0:T(2,128)S(1)} %bitcast.192, pred[512,512]{1,0:T(8,128)(4,1)S(1)} %broadcast_compare_fusion.1), kind=kOutput, calls=%fused_computation.24 | convolution fusion | flops 137363456 | bytes 4988928 | tf_op jit(solution)/shard_map/while/body/eval_jaxpr/cond/branch_1_fun/qhcd,khcd->hcqk/dot_general | solution.py:57
  130.9 3.0 multiply_bitcast_fusion.1
  136.9 10.7 %conditional.8 = ((f32[512,2,2,64]{0,3,2,1:T(8,128)S(1)}, f32[512,2,128]{2,0,1:T(8,128)S(1)})) conditional(s32[]{:T(128)} %convert_element_type.112, (f32[512,2,2,64]{0,3,2,1:T(8,128)S(1)}, f32[512,2,128]{2,0,1:T(8,128)S(1)}) %tuple.152, (s32[]{:T(128)}, s32[]{:T(128)}, s32[512]{0:T(512)S(1)}, bf16[4096,256]{0,1:T(8,128)(2,1)}, ...), branch_computations={%region_9.9_spmd, %region_10.10_spmd} | conditional | flops 547881984 | bytes 43118784 | solution.py:187
  138.3 3.2 %exponential_select_fusion = f32[2,2,512,512]{3,2,1,0:T(8,128)} fusion(bf16[512,2,2,64]{0,3,2,1:T(8,128)(2,1)S(1)} %bitcast.178, bf16[512,2,2,64]{0,3,2,1:T(8,128)(2,1)S(1)} %get-tuple-element.842, f32[2,2,512]{2,1,0:T(2,128)S(1)} %bitcast.192, pred[512,512]{1,0:T(8,128)(4,1)S(1)} %broadcast_compare_fusion.1), kind=kOutput, calls=%fused_computation.24 | convolution fusion | flops 137363456 | bytes 4988928 | tf_op jit(solution)/shard_map/while/body/eval_jaxpr/cond/branch_1_fun/qhcd,khcd->hcqk/dot_general | solution.py:57
  141.5 2.9 multiply_bitcast_fusion.1
  147.6 10.6 %conditional.8 = ((f32[512,2,2,64]{0,3,2,1:T(8,128)S(1)}, f32[512,2,128]{2,0,1:T(8,128)S(1)})) conditional(s32[]{:T(128)} %convert_element_type.112, (f32[512,2,2,64]{0,3,2,1:T(8,128)S(1)}, f32[512,2,128]{2,0,1:T(8,128)S(1)}) %tuple.152, (s32[]{:T(128)}, s32[]{:T(128)}, s32[512]{0:T(512)S(1)}, bf16[4096,256]{0,1:T(8,128)(2,1)}, ...), branch_computations={%region_9.9_spmd, %region_10.10_spmd} | conditional | flops 547881984 | bytes 43118784 | solution.py:187
  149.0 3.2 %exponential_select_fusion = f32[2,2,512,512]{3,2,1,0:T(8,128)} fusion(bf16[512,2,2,64]{0,3,2,1:T(8,128)(2,1)S(1)} %bitcast.178, bf16[512,2,2,64]{0,3,2,1:T(8,128)(2,1)S(1)} %get-tuple-element.842, f32[2,2,512]{2,1,0:T(2,128)S(1)} %bitcast.192, pred[512,512]{1,0:T(8,128)(4,1)S(1)} %broadcast_compare_fusion.1), kind=kOutput, calls=%fused_computation.24 | convolution fusion | flops 137363456 | bytes 4988928 | tf_op jit(solution)/shard_map/while/body/eval_jaxpr/cond/branch_1_fun/qhcd,khcd->hcqk/dot_general | solution.py:57
  152.3 3.0 multiply_bitcast_fusion.1
  158.3 10.6 %conditional.8 = ((f32[512,2,2,64]{0,3,2,1:T(8,128)S(1)}, f32[512,2,128]{2,0,1:T(8,128)S(1)})) conditional(s32[]{:T(128)} %convert_element_type.112, (f32[512,2,2,64]{0,3,2,1:T(8,128)S(1)}, f32[512,2,128]{2,0,1:T(8,128)S(1)}) %tuple.152, (s32[]{:T(128)}, s32[]{:T(128)}, s32[512]{0:T(512)S(1)}, bf16[4096,256]{0,1:T(8,128)(2,1)}, ...), branch_computations={%region_9.9_spmd, %region_10.10_spmd} | conditional | flops 547881984 | bytes 43118784 | solution.py:187
  159.7 3.2 %exponential_select_fusion = f32[2,2,512,512]{3,2,1,0:T(8,128)} fusion(bf16[512,2,2,64]{0,3,2,1:T(8,128)(2,1)S(1)} %bitcast.178, bf16[512,2,2,64]{0,3,2,1:T(8,128)(2,1)S(1)} %get-tuple-element.842, f32[2,2,512]{2,1,0:T(2,128)S(1)} %bitcast.192, pred[512,512]{1,0:T(8,128)(4,1)S(1)} %broadcast_compare_fusion.1), kind=kOutput, calls=%fused_computation.24 | convolution fusion | flops 137363456 | bytes 4988928 | tf_op jit(solution)/shard_map/while/body/eval_jaxpr/cond/branch_1_fun/qhcd,khcd->hcqk/dot_general | solution.py:57
  168.9 10.7 %conditional.8 = ((f32[512,2,2,64]{0,3,2,1:T(8,128)S(1)}, f32[512,2,128]{2,0,1:T(8,128)S(1)})) conditional(s32[]{:T(128)} %convert_element_type.112, (f32[512,2,2,64]{0,3,2,1:T(8,128)S(1)}, f32[512,2,128]{2,0,1:T(8,128)S(1)}) %tuple.152, (s32[]{:T(128)}, s32[]{:T(128)}, s32[512]{0:T(512)S(1)}, bf16[4096,256]{0,1:T(8,128)(2,1)}, ...), branch_computations={%region_9.9_spmd, %region_10.10_spmd} | conditional | flops 547881984 | bytes 43118784 | solution.py:187
  170.3 3.2 %exponential_select_fusion = f32[2,2,512,512]{3,2,1,0:T(8,128)} fusion(bf16[512,2,2,64]{0,3,2,1:T(8,128)(2,1)S(1)} %bitcast.178, bf16[512,2,2,64]{0,3,2,1:T(8,128)(2,1)S(1)} %get-tuple-element.842, f32[2,2,512]{2,1,0:T(2,128)S(1)} %bitcast.192, pred[512,512]{1,0:T(8,128)(4,1)S(1)} %broadcast_compare_fusion.1), kind=kOutput, calls=%fused_computation.24 | convolution fusion | flops 137363456 | bytes 4988928 | tf_op jit(solution)/shard_map/while/body/eval_jaxpr/cond/branch_1_fun/qhcd,khcd->hcqk/dot_general | solution.py:57
  173.5 3.1 %multiply_bitcast_fusion.1 = (f32[2,1,512,512]{3,2,0,1:T(8,128)S(1)}, f32[2,1,512,512]{3,2,0,1:T(8,128)S(1)}) fusion(f32[2,2,512,512]{3,2,1,0:T(8,128)} %exponential_select_fusion, f32[2,512]{1,0:T(2,128)S(1)} %bitcast.189, f32[2,512]{1,0:T(2,128)S(1)} %bitcast.190, f32[2]{0:T(128)S(1)} %neg.16, bf16[512,2,128]{0,2,1:T(8,128)(2,1)S(1)} %bitcast.172, ...), kind=kOutput, calls=%fused_computation.31 | convolution fusion | flops 136839168 | bytes 8921096 | tf_op jit(solution)/shard_map/while/body/eval_jaxpr/cond/branch_1_fun/qhe,khe->hqk/dot_general | solution.py:63
  179.7 10.6 %conditional.8 = ((f32[512,2,2,64]{0,3,2,1:T(8,128)S(1)}, f32[512,2,128]{2,0,1:T(8,128)S(1)})) conditional(s32[]{:T(128)} %convert_element_type.112, (f32[512,2,2,64]{0,3,2,1:T(8,128)S(1)}, f32[512,2,128]{2,0,1:T(8,128)S(1)}) %tuple.152, (s32[]{:T(128)}, s32[]{:T(128)}, s32[512]{0:T(512)S(1)}, bf16[4096,256]{0,1:T(8,128)(2,1)}, ...), branch_computations={%region_9.9_spmd, %region_10.10_spmd} | conditional | flops 547881984 | bytes 43118784 | solution.py:187
  181.1 3.2 %exponential_select_fusion = f32[2,2,512,512]{3,2,1,0:T(8,128)} fusion(bf16[512,2,2,64]{0,3,2,1:T(8,128)(2,1)S(1)} %bitcast.178, bf16[512,2,2,64]{0,3,2,1:T(8,128)(2,1)S(1)} %get-tuple-element.842, f32[2,2,512]{2,1,0:T(2,128)S(1)} %bitcast.192, pred[512,512]{1,0:T(8,128)(4,1)S(1)} %broadcast_compare_fusion.1), kind=kOutput, calls=%fused_computation.24 | convolution fusion | flops 137363456 | bytes 4988928 | tf_op jit(solution)/shard_map/while/body/eval_jaxpr/cond/branch_1_fun/qhcd,khcd->hcqk/dot_general | solution.py:57
  184.3 2.9 multiply_bitcast_fusion.1
  190.3 10.7 %conditional.8 = ((f32[512,2,2,64]{0,3,2,1:T(8,128)S(1)}, f32[512,2,128]{2,0,1:T(8,128)S(1)})) conditional(s32[]{:T(128)} %convert_element_type.112, (f32[512,2,2,64]{0,3,2,1:T(8,128)S(1)}, f32[512,2,128]{2,0,1:T(8,128)S(1)}) %tuple.152, (s32[]{:T(128)}, s32[]{:T(128)}, s32[512]{0:T(512)S(1)}, bf16[4096,256]{0,1:T(8,128)(2,1)}, ...), branch_computations={%region_9.9_spmd, %region_10.10_spmd} | conditional | flops 547881984 | bytes 43118784 | solution.py:187
  191.7 3.2 %exponential_select_fusion = f32[2,2,512,512]{3,2,1,0:T(8,128)} fusion(bf16[512,2,2,64]{0,3,2,1:T(8,128)(2,1)S(1)} %bitcast.178, bf16[512,2,2,64]{0,3,2,1:T(8,128)(2,1)S(1)} %get-tuple-element.842, f32[2,2,512]{2,1,0:T(2,128)S(1)} %bitcast.192, pred[512,512]{1,0:T(8,128)(4,1)S(1)} %broadcast_compare_fusion.1), kind=kOutput, calls=%fused_computation.24 | convolution fusion | flops 137363456 | bytes 4988928 | tf_op jit(solution)/shard_map/while/body/eval_jaxpr/cond/branch_1_fun/qhcd,khcd->hcqk/dot_general | solution.py:57
  195.0 3.0 %multiply_bitcast_fusion.1 = (f32[2,1,512,512]{3,2,0,1:T(8,128)S(1)}, f32[2,1,512,512]{3,2,0,1:T(8,128)S(1)}) fusion(f32[2,2,512,512]{3,2,1,0:T(8,128)} %exponential_select_fusion, f32[2,512]{1,0:T(2,128)S(1)} %bitcast.189, f32[2,512]{1,0:T(2,128)S(1)} %bitcast.190, f32[2]{0:T(128)S(1)} %neg.16, bf16[512,2,128]{0,2,1:T(8,128)(2,1)S(1)} %bitcast.172, ...), kind=kOutput, calls=%fused_computation.31 | convolution fusion | flops 136839168 | bytes 8921096 | tf_op jit(solution)/shard_map/while/body/eval_jaxpr/cond/branch_1_fun/qhe,khe->hqk/dot_general | solution.py:63
  201.2 3.7 %convolution_bitcast_fusion.1 = f32[2048,256]{0,1:T(8,128)} fusion(bf16[512,256]{0,1:T(8,128)(2,1)S(1)} %bitcast.184, bf16[512,2048]{0,1:T(8,128)(2,1)} %bitcast.177), kind=kOutput, calls=%fused_computation.46 | convolution fusion | flops 536870912 | bytes 4456448 | tf_op jit(solution)/shard_map/dot_general | solution.py:197
  207.8 9.2 %all-gather.7.cloned.1.call-done = bf16[4096,256]{0,1:T(8,128)(2,1)} async-done(((bf16[512,256]{0,1:T(8,128)(2,1)}), bf16[4096,256]{0,1:T(8,128)(2,1)}) %all-gather.7.cloned.1.call-update) | async-done | bytes 2097168 | tf_op jit(solution)/shard_map/all_gather | solution.py:100
  217.1 4.3 %while.38 = (s32[]{:T(128)}, f32[512,2,2,64]{0,3,2,1:T(8,128)S(1)}, s32[]{:T(128)}, bf16[4096,256]{0,1:T(8,128)(2,1)}, bf16[512,2,2,64]{0,3,2,1:T(8,128)(2,1)S(1...) while((s32[]{:T(128)}, f32[512,2,2,64]{0,3,2,1:T(8,128)S(1)}, ...), condition=%wide.region_7.8_spmd.clone, body=%wide.region_4.7_spmd.clone.sunk | while | flops 411960320 | bytes 20756812 | solution.py:135
  217.2 3.9 %conditional.7 = (f32[512,2,2,64]{0,3,2,1:T(8,128)S(1)}) conditional(s32[]{:T(128)} %convert_element_type.111, f32[512,2,2,64]{0,3,2,1:T(8,128)S(1)} %get-tuple-element.1245, (s32[]{:T(128)}, s32[512]{0:T(512)S(1)}, s32[]{:T(128)}, bf16[4096,256]{0,1:T(8,128)(2,1)}, bf16[512,2,2,64]{0,3,2,1:T(8,128)(2,1)S(1)}, /*index=5*/f32[512,2,2]{0,2,1:T(2,128)S(1)}, ...), branch_computations={%region_5.0_spmd, %region_6.6_spmd} | conditional | flops 411960320 | bytes 20754510 | solution.py:133
  222.4 65.2 %reduce-scatter.2.cloned.1.call-done = f32[256,256]{0,1:T(8,128)} async-done(((f32[2048,256]{0,1:T(8,128)}), f32[256,256]{0,1:T(8,128)}) %reduce-scatter.2.cloned.1.call-update) | async-done | bytes 262160 | tf_op jit(solution)/shard_map/reduce_scatter | solution.py:196
  (223 shorter events, 64.1 us)
Async XLA Ops:
  7.2 40.4 %copy-start = (bf16[2048,256]{1,0:T(8,128)(2,1)S(1)}, bf16[2048,256]{1,0:T(8,128)(2,1)}, u32[]{:S(2)}) copy-start(bf16[2048,256]{1,0:T(8,128)(2,1)} %param.20) | copy-start | bytes 3145732
  7.2 4.4 %copy-start.11 = (f32[128]{0:T(128)S(1)}, f32[128]{0:T(128)}, u32[]{:S(2)}) copy-start(f32[128]{0:T(128)} %param.25) | copy-start | bytes 1540
  7.2 4.4 %copy-start.8 = (f32[2]{0:T(128)S(1)}, f32[2]{0:T(128)}, u32[]{:S(2)}) copy-start(f32[2]{0:T(128)} %param.24) | copy-start | bytes 28
  7.2 105.3 %all-gather.9.cloned.1.call-start = ((), (), s32[]{:S(2)}) async-start(), calls=%async_computation.4 | async-start | bytes 2359296 | tf_op jit(solution)/shard_map/all_gather | solution.py:137
  9.1 106.2 %all-gather.11.cloned.1.call-start = ((), (), s32[]{:S(2)}) async-start(), calls=%async_computation.5 | async-start | bytes 2359296 | tf_op jit(solution)/shard_map/all_gather | solution.py:138
  13.1 194.7 %all-gather.5.cloned.1.call-start = ((), (), s32[]{:S(2)}) async-start(), calls=%async_computation.2 | async-start | bytes 2359296 | tf_op jit(solution)/shard_map/all_gather | solution.py:99
  15.0 202.1 %all-gather.7.cloned.1.call-start = ((), (), s32[]{:S(2)}) async-start(), calls=%async_computation.3 | async-start | bytes 2359296 | tf_op jit(solution)/shard_map/all_gather | solution.py:100
  46.2 1.4 copy-start.2
  49.0 1.2 copy-start.7
  49.0 63.3 %copy-start.6 = (bf16[512,256]{0,1:T(8,128)(2,1)S(1)}, bf16[512,256]{0,1:T(8,128)(2,1)}, u32[]{:S(2)}) copy-start(bf16[512,256]{0,1:T(8,128)(2,1)} %convolution_convert_fusion) | copy-start | bytes 786436
  49.0 66.4 %copy-start.5 = (bf16[512,256]{0,1:T(8,128)(2,1)S(1)}, bf16[512,256]{0,1:T(8,128)(2,1)}, u32[]{:S(2)}) copy-start(bf16[512,256]{0,1:T(8,128)(2,1)} %copy.47) | copy-start | bytes 786436
  49.1 238.6 %reduce-scatter.2.cloned.1.call-start = ((), (), s32[]{:S(2)}) async-start(), calls=%async_computation.6 | async-start | bytes 2359296 | tf_op jit(solution)/shard_map/reduce_scatter | solution.py:196
  116.9 3.2 %copy-start.9 = (f32[2]{0:T(128)S(1)}, f32[2]{0:T(128)}, u32[]{:S(2)}) copy-start(f32[2]{0:T(128)} %get-tuple-element.847) | copy-start | bytes 28 | tf_op jit(solution)/shard_map/while/body/eval_jaxpr/cond
  123.1 2.3 copy-start.1
  127.6 3.2 %copy-start.9 = (f32[2]{0:T(128)S(1)}, f32[2]{0:T(128)}, u32[]{:S(2)}) copy-start(f32[2]{0:T(128)} %get-tuple-element.847) | copy-start | bytes 28 | tf_op jit(solution)/shard_map/while/body/eval_jaxpr/cond
  133.8 2.2 copy-start.1
  138.3 3.2 %copy-start.9 = (f32[2]{0:T(128)S(1)}, f32[2]{0:T(128)}, u32[]{:S(2)}) copy-start(f32[2]{0:T(128)} %get-tuple-element.847) | copy-start | bytes 28 | tf_op jit(solution)/shard_map/while/body/eval_jaxpr/cond
  144.5 2.3 copy-start.1
  149.0 3.2 %copy-start.9 = (f32[2]{0:T(128)S(1)}, f32[2]{0:T(128)}, u32[]{:S(2)}) copy-start(f32[2]{0:T(128)} %get-tuple-element.847) | copy-start | bytes 28 | tf_op jit(solution)/shard_map/while/body/eval_jaxpr/cond
  155.2 2.2 copy-start.1
  159.7 3.2 %copy-start.9 = (f32[2]{0:T(128)S(1)}, f32[2]{0:T(128)}, u32[]{:S(2)}) copy-start(f32[2]{0:T(128)} %get-tuple-element.847) | copy-start | bytes 28 | tf_op jit(solution)/shard_map/while/body/eval_jaxpr/cond
  165.9 2.2 copy-start.1
  170.3 3.2 %copy-start.9 = (f32[2]{0:T(128)S(1)}, f32[2]{0:T(128)}, u32[]{:S(2)}) copy-start(f32[2]{0:T(128)} %get-tuple-element.847) | copy-start | bytes 28 | tf_op jit(solution)/shard_map/while/body/eval_jaxpr/cond
  176.6 2.2 copy-start.1
  181.1 3.2 %copy-start.9 = (f32[2]{0:T(128)S(1)}, f32[2]{0:T(128)}, u32[]{:S(2)}) copy-start(f32[2]{0:T(128)} %get-tuple-element.847) | copy-start | bytes 28 | tf_op jit(solution)/shard_map/while/body/eval_jaxpr/cond
  187.3 2.2 copy-start.1
  191.7 3.2 %copy-start.9 = (f32[2]{0:T(128)S(1)}, f32[2]{0:T(128)}, u32[]{:S(2)}) copy-start(f32[2]{0:T(128)} %get-tuple-element.847) | copy-start | bytes 28 | tf_op jit(solution)/shard_map/while/body/eval_jaxpr/cond
  198.0 2.2 copy-start.1
  204.9 1.0 copy-start.3
  204.9 12.2 %copy-start.4 = (bf16[512,256]{0,1:T(8,128)(2,1)S(1)}, bf16[512,256]{0,1:T(8,128)(2,1)}, u32[]{:S(2)}) copy-start(bf16[512,256]{0,1:T(8,128)(2,1)} %copy.48) | copy-start | bytes 786436
  204.9 12.2 %copy-start.10 = (f32[2]{0:T(128)S(1)}, f32[2]{0:T(128)}, u32[]{:S(2)}) copy-start(f32[2]{0:T(128)} %get-tuple-element.1336) | copy-start | bytes 28
Sparse Core Ops, SparseCore 0:
  10.6 53.2 all-gather.8
  66.5 48.7 all-gather.10
  118.0 48.5 all-gather.4
  168.5 48.5 all-gather.6
  220.4 67.1 reduce-scatter.1
